TPU v7x, 32 devices: a whole 2x2x4 slice. The times are simulated.
32 devices in a mesh: rep: 2 (over x), fs: 4 (over z), tp: 4 (over y, core).
Axes of the slice: x: 2, y: 2, z: 4, core: 2. Of those that a mesh axis runs over, the one named last changes fastest.
Arguments:
- tokens: bfloat16 [4096, 2048], P(('rep', 'fs', 'tp')), may hold values from -6 to 6
- norm_gain: float32 [2048], replicated, may hold values from 0.1 to 1.9
- gate_weight: float32 [2048, 5632], P('fs', 'tp'), may hold values from -0.125 to 0.125
- gate_scale: float32 [5632], P('tp'), may hold values from 0.5 to 2
- up_weight: float32 [2048, 5632], P('fs', 'tp'), may hold values from -0.125 to 0.125
- up_scale: float32 [5632], P('tp'), may hold values from 0.5 to 2
- down_weight: float32 [5632, 2048], P('tp', 'fs'), may hold values from -0.078125 to 0.078125
- down_scale: float32 [2048], P('fs'), may hold values from 0.5 to 2
Outputs:
- mixed: bfloat16 [4096, 2048], P(('rep', 'fs', 'tp'))
All inputs are finite; a program needn't handle non-finite values.
Results may differ from a plain program's by a relative error of at most 0.014.
Values may be sent and summed in bfloat16 or wider, within the bound.
A program may use at most 64 MiB of HBM per device.

v0:
```python
import jax
import jax.numpy as jnp
from jax import lax
from jax.sharding import PartitionSpec as P


def shards(
    tokens, norm_gain, gate_weight, gate_scale, up_weight, up_scale, down_weight, down_scale
):
    flat = tokens.astype(jnp.float32)
    mean_square = jnp.mean(flat * flat, axis=-1, keepdims=True)
    inverse = lax.rsqrt(mean_square + 1e-06)
    normed = (flat * inverse * norm_gain).astype(jnp.bfloat16)
    group = lax.all_gather(normed, "tp", axis=0, tiled=True)
    gate_low = gate_weight.astype(jnp.bfloat16)
    up_low = up_weight.astype(jnp.bfloat16)
    down_low = down_weight.astype(jnp.bfloat16)
    gate = jnp.dot(
        group,
        lax.all_gather(gate_low, "fs", axis=0, tiled=True),
        preferred_element_type=jnp.float32,
    )
    up = jnp.dot(
        group, lax.all_gather(up_low, "fs", axis=0, tiled=True), preferred_element_type=jnp.float32
    )
    down_full = lax.all_gather(down_low, "fs", axis=1, tiled=True)
    gate = gate * gate_scale
    up = up * up_scale
    hidden = (jax.nn.silu(gate) * up).astype(jnp.bfloat16)
    scales = lax.all_gather(down_scale, "fs", axis=0, tiled=True)
    total = lax.psum_scatter(
        jnp.dot(hidden, down_full, preferred_element_type=jnp.float32).astype(jnp.bfloat16),
        "tp",
        scatter_dimension=0,
        tiled=True,
    ).astype(jnp.float32)
    return (total * scales).astype(jnp.bfloat16)


def solution(mesh):
    in_specs = (
        P(("rep", "fs", "tp"), None),
        P(),
        P("fs", "tp"),
        P("tp"),
        P("fs", "tp"),
        P("tp"),
        P("tp", "fs"),
        P("fs"),
    )
    out_specs = P(("rep", "fs", "tp"), None)
    return jax.shard_map(shards, mesh=mesh, in_specs=in_specs, out_specs=out_specs, check_vma=False)
```

profile of v0, /device:TPU:0, one launch (start us, length us, event | category | flops | bytes accessed | tf_op | source)
XLA Modules:
  0.0 408.0 jit_solution(18322760977833249545)
XLA Ops:
  6.5 0.0 all-gather.6.cloned.1.call-start
  6.5 1.2 fusion.2
  7.8 2.0 fusion.4
  9.8 0.0 all-gather.6.cloned.1.call-update
  9.8 0.0 copy-start
  9.8 0.0 all-gather.8.cloned.1.call-start
  9.9 3.3 convert_element_type.29
  13.2 0.0 all-gather.8.cloned.1.call-update
  13.2 0.0 all-gather.10.cloned.1.call-start
  13.2 0.0 copy-done
  13.2 1.3 convert_element_type.30
  14.5 0.0 all-gather.10.cloned.1.call-update
  14.5 0.0 copy-start.3
  14.6 0.0 all-gather.12.cloned.1.call-start
  14.6 3.1 convert_element_type.32
  17.8 0.0 all-gather.12.cloned.1.call-update
  17.8 0.0 copy-start.4
  17.8 0.0 reduce-scatter.2.cloned.1.call-start
  17.8 17.4 %all-gather.6.cloned.1.call-done = bf16[512,2048]{1,0:T(8,128)(2,1)} async-done(((bf16[128,2048]{1,0:T(8,128)(2,1)}), bf16[512,2048]{1,0:T(8,128)(2,1)}) %all-gather.6.cloned.1.call-update) | async-done | bytes 2097168 | tf_op jit(solution)/shard_map/all_gather | solution.py:14
  35.3 108.3 %all-gather.8.cloned.1.call-done = bf16[2048,1408]{1,0:T(8,128)(2,1)} async-done(((bf16[512,1408]{1,0:T(8,128)(2,1)}), bf16[2048,1408]{1,0:T(8,128)(2,1)}) %all-gather.8.cloned.1.call-update) | async-done | bytes 5767184 | tf_op jit(solution)/shard_map/all_gather | solution.py:20
  143.6 0.0 copy-done.3
  143.6 8.2 %convolution_multiply_fusion.1 = f32[512,1408]{1,0:T(8,128)} fusion(bf16[512,2048]{1,0:T(8,128)(2,1)} %all-gather.6.cloned.1.call-done, bf16[2048,1408]{1,0:T(8,128)(2,1)} %all-gather.8.cloned.1.call-done, f32[1408]{0:T(1024)S(1)} %copy-done.3), kind=kOutput, calls=%fused_computation.2 | convolution fusion | flops 2953510912 | bytes 10753536 | tf_op jit(solution)/shard_map/dot_general | solution.py:18
  151.8 98.3 %all-gather.10.cloned.1.call-done = bf16[2048,1408]{1,0:T(8,128)(2,1)} async-done(((bf16[512,1408]{1,0:T(8,128)(2,1)}), bf16[2048,1408]{1,0:T(8,128)(2,1)}) %all-gather.10.cloned.1.call-update) | async-done | bytes 5767184 | tf_op jit(solution)/shard_map/all_gather | solution.py:24
  250.1 106.4 %all-gather.12.cloned.1.call-done = bf16[1408,2048]{1,0:T(8,128)(2,1)} async-done(((bf16[1408,512]{1,0:T(8,128)(2,1)}), bf16[1408,2048]{1,0:T(8,128)(2,1)}) %all-gather.12.cloned.1.call-update) | async-done | bytes 5767184 | tf_op jit(solution)/shard_map/all_gather | solution.py:26
  356.5 0.0 copy-done.4
  356.5 0.0 copy-done.2
  356.5 13.4 %convolution_convert_fusion = bf16[512,2048]{1,0:T(8,128)(2,1)} fusion(bf16[1408,2048]{1,0:T(8,128)(2,1)} %all-gather.12.cloned.1.call-done, bf16[512,2048]{1,0:T(8,128)(2,1)S(1)} %copy-done.2, bf16[2048,1408]{1,0:T(8,128)(2,1)} %all-gather.10.cloned.1.call-done, f32[512,1408]{1,0:T(8,128)} %convolution_multiply_fusion.1, f32[1408]{0:T(1024)S(1)} %copy-done.4), kind=kOutput, calls=%fused_computation.4 | convolution fusion | flops 5911674880 | bytes 18617856 | tf_op jit(solution)/shard_map/dot_general | solution.py:32
  370.0 0.0 reduce-scatter.2.cloned.1.call-update
  370.0 0.0 copy-done.1
  370.0 11.9 %all-gather = f32[4,1,512]{2,1,0:T(1,128)S(1)} all-gather(f32[1,1,512]{2,1,0:T(1,128)S(1)} %bitcast.8), channel_id=1, replica_groups=mesh['rep'=2,'fs'=4,'tp'=4] {'fs'}, dimensions={0}, use_global_device_ids=true | all-gather | bytes 10240 | tf_op jit(solution)/shard_map/all_gather | solution.py:30
  381.9 17.6 %reduce-scatter.2.cloned.1.call-done = bf16[128,2048]{1,0:T(8,128)(2,1)} async-done(((bf16[512,2048]{1,0:T(8,128)(2,1)}), bf16[128,2048]{1,0:T(8,128)(2,1)}) %reduce-scatter.2.cloned.1.call-update) | async-done | bytes 524304 | tf_op jit(solution)/shard_map/reduce_scatter | solution.py:31
  399.6 1.9 multiply_convert_fusion
  (3 shorter events, 0.0 us)
Async XLA Ops:
  6.5 28.7 %all-gather.6.cloned.1.call-start = ((), (), s32[]{:S(2)}) async-start(), calls=%async_computation.1 | async-start | bytes 2621440 | tf_op jit(solution)/shard_map/all_gather | solution.py:14
  9.8 3.4 copy-start
  9.8 133.7 %all-gather.8.cloned.1.call-start = ((), (), s32[]{:S(2)}) async-start(), calls=%async_computation.2 | async-start | bytes 7208960 | tf_op jit(solution)/shard_map/all_gather | solution.py:20
  13.2 236.9 %all-gather.10.cloned.1.call-start = ((), (), s32[]{:S(2)}) async-start(), calls=%async_computation.3 | async-start | bytes 7208960 | tf_op jit(solution)/shard_map/all_gather | solution.py:24
  14.5 129.0 %copy-start.3 = (f32[1408]{0:T(1024)S(1)}, f32[1408]{0:T(1024)}, u32[]{:S(2)}) copy-start(f32[1408]{0:T(1024)} %param.11) | copy-start | bytes 16900
  14.6 342.0 %all-gather.12.cloned.1.call-start = ((), (), s32[]{:S(2)}) async-start(), calls=%async_computation.4 | async-start | bytes 7208960 | tf_op jit(solution)/shard_map/all_gather | solution.py:26
  17.8 338.7 %copy-start.4 = (f32[1408]{0:T(1024)S(1)}, f32[1408]{0:T(1024)}, u32[]{:S(2)}) copy-start(f32[1408]{0:T(1024)} %param.13) | copy-start | bytes 16900
  17.8 381.8 %reduce-scatter.2.cloned.1.call-start = ((), (), s32[]{:S(2)}) async-start(), calls=%async_computation.5 | async-start | bytes 2621440 | tf_op jit(solution)/shard_map/reduce_scatter | solution.py:31
  35.3 321.2 %copy-start.2 = (bf16[512,2048]{1,0:T(8,128)(2,1)S(1)}, bf16[512,2048]{1,0:T(8,128)(2,1)}, u32[]{:S(2)}) copy-start(bf16[512,2048]{1,0:T(8,128)(2,1)} %all-gather.6.cloned.1.call-done) | copy-start | bytes 6291460
  151.8 218.2 %copy-start.1 = (f32[512]{0:T(512)S(1)}, f32[512]{0:T(512)}, u32[]{:S(2)}) copy-start(f32[512]{0:T(512)} %param.15) | copy-start | bytes 6148
Sparse Core Ops, SparseCore 0:
  9.9 25.2 all-gather.5
  36.8 106.6 all-gather.7
  145.1 104.9 all-gather.9
  251.5 104.9 all-gather.11
  370.1 29.4 reduce-scatter.1
where the time goes:
time: 408 us
  waiting for transfers between devices  348 us (85%)
  matrix products  21.7 us (5%)
  between operations  13.2 us (3%)
  other arithmetic  12.9 us (3%)
  blocking collectives  11.9 us (3%)
    all_gather x1, waiting for transfers between devices, shards(): lax.all_gather(gate_low, 'fs', axis=0, tiled=True)  108 us
    all_gather x1, waiting for transfers between devices, shards(): down_full = lax.all_gather(down_low, 'fs', axis=1, tiled=True)  106 us
    all_gather x1, waiting for transfers between devices, shards(): lax.all_gather(up_low, 'fs', axis=0, tiled=True)  98.3 us
    reduce_scatter x1, waiting for transfers between devices, shards(): lax.psum_scatter(jnp.dot(hidden, down_full, preferred_element_type=jnp.fl...  17.6 us
    all_gather x1, waiting for transfers between devices, shards(): group = lax.all_gather(normed, 'tp', axis=0, tiled=True)  17.4 us
    dot_general x1, matrix products, shards(): jnp.dot(hidden, down_full, preferred_element_type=jnp.float32)  13.4 us
    all_gather x1, blocking collectives, shards(): scales = lax.all_gather(down_scale, 'fs', axis=0, tiled=True)  11.9 us
    dot_general x1, matrix products, shards(): jnp.dot(group, lax.all_gather(gate_low, 'fs', axis=0, tiled=True), prefer...  8.23 us
  transfers between devices with their start and end apart: 5, of which 5 were waited for; matrix products, arithmetic and copies ran while one was open for 4% of the time, Pallas kernels for 0%

commit v1 on v0

--- a/solution.py
+++ b/solution.py
@@ -7,14 +7,22 @@
 def shards(
     tokens, norm_gain, gate_weight, gate_scale, up_weight, up_scale, down_weight, down_scale
 ):
+    n_rep = lax.axis_size("rep")
+    rep = lax.axis_index("rep")
+    width = gate_weight.shape[1] // n_rep
+    start = rep * width
+
+    def part(array, axis):
+        return lax.dynamic_slice_in_dim(array, start, width, axis)
+
     flat = tokens.astype(jnp.float32)
     mean_square = jnp.mean(flat * flat, axis=-1, keepdims=True)
     inverse = lax.rsqrt(mean_square + 1e-06)
     normed = (flat * inverse * norm_gain).astype(jnp.bfloat16)
-    group = lax.all_gather(normed, "tp", axis=0, tiled=True)
-    gate_low = gate_weight.astype(jnp.bfloat16)
-    up_low = up_weight.astype(jnp.bfloat16)
-    down_low = down_weight.astype(jnp.bfloat16)
+    group = lax.all_gather(normed, ("rep", "tp"), axis=0, tiled=True)
+    gate_low = part(gate_weight, 1).astype(jnp.bfloat16)
+    up_low = part(up_weight, 1).astype(jnp.bfloat16)
+    down_low = part(down_weight, 0).astype(jnp.bfloat16)
     gate = jnp.dot(
         group,
         lax.all_gather(gate_low, "fs", axis=0, tiled=True),
@@ -24,13 +32,13 @@
         group, lax.all_gather(up_low, "fs", axis=0, tiled=True), preferred_element_type=jnp.float32
     )
     down_full = lax.all_gather(down_low, "fs", axis=1, tiled=True)
-    gate = gate * gate_scale
-    up = up * up_scale
+    gate = gate * part(gate_scale, 0)
+    up = up * part(up_scale, 0)
     hidden = (jax.nn.silu(gate) * up).astype(jnp.bfloat16)
     scales = lax.all_gather(down_scale, "fs", axis=0, tiled=True)
     total = lax.psum_scatter(
         jnp.dot(hidden, down_full, preferred_element_type=jnp.float32).astype(jnp.bfloat16),
-        "tp",
+        ("rep", "tp"),
         scatter_dimension=0,
         tiled=True,
     ).astype(jnp.float32)

time: 408 us -> 308 us (0.75)
  waiting for transfers between devices: 348 us -> 250 us
  local copies, waits for them, and re-layouts: 0.03 us -> 8.92 us
  other arithmetic: 12.9 us -> 4.16 us
    all_gather x1, waiting for transfers between devices: 108 us -> 58.6 us  [shards(): lax.all_gather(gate_low, 'fs', axis=0, tiled=True)]
    all_gather x1, waiting for transfers between devices: 106 us -> 59.2 us  [shards(): down_full = lax.all_gather(down_low, 'fs', axis=1, tiled=True)]
    all_gather x1, waiting for transfers between devices: 98.3 us -> 57.1 us  [shards(): lax.all_gather(up_low, 'fs', axis=0, tiled=True)]
    reduce_scatter x1, waiting for transfers between devices: 17.6 us -> 37.4 us  [shards(): lax.psum_scatter(jnp.dot(hidden, down_full, preferred_element_type=jnp.fl...]
    all_gather x1, waiting for transfers between devices: 17.4 us -> 37.1 us  [shards(): group = lax.all_gather(normed, ('rep', 'tp'), axis=0, tiled=True)]
    convert_element_type x3 -> x0, other arithmetic: 7.69 us -> none  [the longest x1 3.27 us: shards(): gate_low = gate_weight.astype(jnp.bfloat16)]
    convert_element_type x0 -> x3, local copies, waits for them, and re-layouts: none -> 6.29 us  [the longest x1 2.74 us: shards(): up_low = part(up_weight, 1).astype(jnp.bfloat16)]
  transfers between devices with their start and end apart: 5 -> 5, of which waited for: 5 -> 5; matrix products, arithmetic and copies ran while one was open for 4% -> 5% of each run, Pallas kernels for 0% -> 0%
where the time goes in v1:
time: 308 us
  waiting for transfers between devices  250 us (81%)
  matrix products  20.2 us (7%)
  between operations  13.2 us (4%)
  blocking collectives  11.9 us (4%)
  local copies, waits for them, and re-layouts  8.92 us (3%)
  other arithmetic  4.16 us (1%)
    all_gather x1, waiting for transfers between devices, shards(): down_full = lax.all_gather(down_low, 'fs', axis=1, tiled=True)  59.2 us
    all_gather x1, waiting for transfers between devices, shards(): lax.all_gather(gate_low, 'fs', axis=0, tiled=True)  58.6 us
    all_gather x1, waiting for transfers between devices, shards(): lax.all_gather(up_low, 'fs', axis=0, tiled=True)  57.1 us
    reduce_scatter x1, waiting for transfers between devices, shards(): lax.psum_scatter(jnp.dot(hidden, down_full, preferred_element_type=jnp.fl...  37.4 us
    all_gather x1, waiting for transfers between devices, shards(): group = lax.all_gather(normed, ('rep', 'tp'), axis=0, tiled=True)  37.1 us
    dot_general x1, matrix products, shards(): jnp.dot(hidden, down_full, preferred_element_type=jnp.float32)  12.3 us
    all_gather x1, blocking collectives, shards(): scales = lax.all_gather(down_scale, 'fs', axis=0, tiled=True)  11.9 us
    dot_general x1, matrix products, shards(): jnp.dot(group, lax.all_gather(gate_low, 'fs', axis=0, tiled=True), prefer...  7.9 us
  transfers between devices with their start and end apart: 5, of which 5 were waited for; matrix products, arithmetic and copies ran while one was open for 5% of the time, Pallas kernels for 0%

profile of v1, /device:TPU:0, one launch (start us, length us, event | category | flops | bytes accessed | tf_op | source)
XLA Modules:
  0.0 308.1 jit_solution(6207909742359432319)
XLA Ops:
  6.5 0.0 copy-start
  6.5 0.0 all-gather.8.cloned.1.call-start
  6.6 1.8 copy-done
  8.4 1.2 dynamic-slice_convert_fusion.1
  9.6 0.0 all-gather.8.cloned.1.call-update
  9.6 0.0 all-gather.6.cloned.1.call-start
  9.7 1.2 fusion
  10.9 0.0 copy-done.1
  10.9 0.0 copy-start.4
  10.9 0.0 copy-start.5
  10.9 1.0 fusion.2
  11.9 0.0 all-gather.6.cloned.1.call-update
  11.9 0.0 all-gather.10.cloned.1.call-start
  12.0 2.7 dynamic-slice_convert_fusion
  14.7 0.0 all-gather.10.cloned.1.call-update
  14.8 0.0 all-gather.12.cloned.1.call-start
  14.8 2.3 dynamic-slice_convert_fusion.2
  17.1 0.0 all-gather.12.cloned.1.call-update
  17.2 0.0 reduce-scatter.2.cloned.1.call-start
  17.2 0.1 dynamic_slice.16
  17.3 0.1 dynamic_slice.18
  17.4 58.6 %all-gather.8.cloned.1.call-done = bf16[2048,704]{1,0:T(8,128)(2,1)} async-done(((bf16[512,704]{1,0:T(8,128)(2,1)}), bf16[2048,704]{1,0:T(8,128)(2,1)}) %all-gather.8.cloned.1.call-update) | async-done | bytes 2883600 | tf_op jit(solution)/shard_map/all_gather | solution.py:28
  75.9 37.1 %all-gather.6.cloned.1.call-done = bf16[1024,2048]{1,0:T(8,128)(2,1)} async-done(((bf16[128,2048]{1,0:T(8,128)(2,1)}), bf16[1024,2048]{1,0:T(8,128)(2,1)}) %all-gather.6.cloned.1.call-update) | async-done | bytes 4194320 | tf_op jit(solution)/shard_map/all_gather | solution.py:22
  113.1 7.9 %fusion.4 = f32[1024,704]{0,1:T(8,128)} fusion(bf16[1024,2048]{1,0:T(8,128)(2,1)} %all-gather.6.cloned.1.call-done, bf16[2048,704]{1,0:T(8,128)(2,1)} %all-gather.8.cloned.1.call-done), kind=kOutput, calls=%fused_computation.13 | convolution fusion | flops 2952790016 | bytes 9961472 | tf_op jit(solution)/shard_map/dot_general | solution.py:26
  121.0 57.1 %all-gather.10.cloned.1.call-done = bf16[2048,704]{1,0:T(8,128)(2,1)} async-done(((bf16[512,704]{1,0:T(8,128)(2,1)}), bf16[2048,704]{1,0:T(8,128)(2,1)}) %all-gather.10.cloned.1.call-update) | async-done | bytes 2883600 | tf_op jit(solution)/shard_map/all_gather | solution.py:32
  178.1 59.2 %all-gather.12.cloned.1.call-done = bf16[704,2048]{1,0:T(8,128)(2,1)} async-done(((bf16[704,512]{1,0:T(8,128)(2,1)}), bf16[704,2048]{1,0:T(8,128)(2,1)}) %all-gather.12.cloned.1.call-update) | async-done | bytes 2883600 | tf_op jit(solution)/shard_map/all_gather | solution.py:34
  237.3 12.3 %convolution_convert_fusion = bf16[1024,2048]{1,0:T(8,128)(2,1)} fusion(bf16[704,2048]{1,0:T(8,128)(2,1)} %all-gather.12.cloned.1.call-done, f32[1024,704]{0,1:T(8,128)} %fusion.4, bf16[1024,2048]{1,0:T(8,128)(2,1)} %all-gather.6.cloned.1.call-done, bf16[2048,704]{1,0:T(8,128)(2,1)} %all-gather.10.cloned.1.call-done, f32[704]{0:T(1024)S(1)} %dynamic_slice.18, ...), kind=kOutput, calls=%fused_computation | convolution fusion | flops 5913444352 | bytes 17044992 | tf_op jit(solution)/shard_map/dot_general | solution.py:40
  249.7 0.0 reduce-scatter.2.cloned.1.call-update
  249.7 0.7 copy-done.3
  250.3 11.9 %all-gather = f32[4,1,512]{2,1,0:T(1,128)S(1)} all-gather(f32[1,1,512]{2,1,0:T(1,128)S(1)} %bitcast.8), channel_id=1, replica_groups=mesh['rep'=2,'fs'=4,'tp'=4] {'fs'}, dimensions={0}, use_global_device_ids=true | all-gather | bytes 10240 | tf_op jit(solution)/shard_map/all_gather | solution.py:38
  262.3 37.4 %reduce-scatter.2.cloned.1.call-done = bf16[128,2048]{1,0:T(8,128)(2,1)} async-done(((bf16[1024,2048]{1,0:T(8,128)(2,1)}), bf16[128,2048]{1,0:T(8,128)(2,1)}) %reduce-scatter.2.cloned.1.call-update) | async-done | bytes 524304 | tf_op jit(solution)/shard_map/reduce_scatter | solution.py:39
  299.7 1.9 multiply_convert_fusion.1
  (7 shorter events, 0.0 us)
Async XLA Ops:
  6.5 1.8 copy-start
  6.5 4.4 %copy-start.1 = (bf16[128,2048]{1,0:T(8,128)(2,1)S(1)}, bf16[128,2048]{1,0:T(8,128)(2,1)}, u32[]{:S(2)}) copy-start(bf16[128,2048]{1,0:T(8,128)(2,1)} %param.8) | copy-start | bytes 1572868
  6.5 4.4 %copy-start.2 = (f32[2048]{0:T(1024)S(1)}, f32[2048]{0:T(1024)}, u32[]{:S(2)}) copy-start(f32[2048]{0:T(1024)} %param.9) | copy-start | bytes 24580
  6.5 69.4 %all-gather.8.cloned.1.call-start = ((), (), s32[]{:S(2)}) async-start(), calls=%async_computation.2 | async-start | bytes 3932160 | tf_op jit(solution)/shard_map/all_gather | solution.py:28
  9.6 103.5 %all-gather.6.cloned.1.call-start = ((), (), s32[]{:S(2)}) async-start(), calls=%async_computation.1 | async-start | bytes 4718592 | tf_op jit(solution)/shard_map/all_gather | solution.py:22
  10.9 6.3 %copy-start.4 = (f32[1408]{0:T(1024)S(1)}, f32[1408]{0:T(1024)}, u32[]{:S(2)}) copy-start(f32[1408]{0:T(1024)} %param.11) | copy-start | bytes 16900
  10.9 6.4 %copy-start.5 = (f32[1408]{0:T(1024)S(1)}, f32[1408]{0:T(1024)}, u32[]{:S(2)}) copy-start(f32[1408]{0:T(1024)} %param.13) | copy-start | bytes 16900
  11.9 166.2 %all-gather.10.cloned.1.call-start = ((), (), s32[]{:S(2)}) async-start(), calls=%async_computation.3 | async-start | bytes 3932160 | tf_op jit(solution)/shard_map/all_gather | solution.py:32
  14.8 222.6 %all-gather.12.cloned.1.call-start = ((), (), s32[]{:S(2)}) async-start(), calls=%async_computation.4 | async-start | bytes 3604480 | tf_op jit(solution)/shard_map/all_gather | solution.py:34
  17.2 282.5 %reduce-scatter.2.cloned.1.call-start = ((), (), s32[]{:S(2)}) async-start(), calls=%async_computation.5 | async-start | bytes 4718592 | tf_op jit(solution)/shard_map/reduce_scatter | solution.py:39
  249.7 0.7 copy-start.3
Sparse Core Ops, SparseCore 0:
  9.7 66.1 all-gather.7
  77.8 35.2 all-gather.5
  114.7 63.4 all-gather.9
  179.6 57.7 all-gather.11
  249.8 49.8 reduce-scatter.1

commit v2 on v0

v2 whole, which is shorter than its diff:
```python
import functools

import jax
import jax.numpy as jnp
from jax import lax
from jax.experimental import pallas as pl
from jax.experimental.pallas import tpu as pltpu
from jax.sharding import PartitionSpec as P

MESH = pl.DeviceIdType.MESH


def layer(
    n_rep,
    n_fs,
    n_tp,
    tok_ref,
    gu_ref,
    dn_ref,
    gs_ref,
    us_ref,
    ds_ref,
    out_ref,
    tok_all,
    gu_all,
    dn_all,
    sc_all,
    acc,
    hidden,
    parts,
    landed,
    tok_send,
    tok_recv,
    gu_send,
    gu_recv,
    dn_send,
    dn_recv,
    sc_send,
    sc_recv,
    part_send,
    part_recv,
):
    rep, fs, tp = lax.axis_index("rep"), lax.axis_index("fs"), lax.axis_index("tp")
    peers = n_rep * n_tp
    me = rep * n_tp + tp
    rows = tok_ref.shape[0]
    depth = gu_ref.shape[0]
    half = gu_ref.shape[1] // 2
    cols = dn_ref.shape[1]
    last = n_fs - 1

    def plane(peer):
        return (peer // n_tp, fs, peer % n_tp)

    barrier = pltpu.get_barrier_semaphore()
    for hop in (1, n_fs - 1):
        pl.semaphore_signal(
            barrier, inc=1, device_id=(rep, (fs + hop) % n_fs, tp), device_id_type=MESH
        )
    for hop in range(1, peers):
        pl.semaphore_signal(
            barrier, inc=1, device_id=plane((me + hop) % peers), device_id_type=MESH
        )
    pl.semaphore_wait(barrier, peers + 1)

    def side(own, store, send, recv, source, way, first):
        return pltpu.make_async_remote_copy(
            src_ref=own if first else store.at[source],
            dst_ref=store.at[source],
            send_sem=send.at[way, source],
            recv_sem=recv.at[source],
            device_id=(rep, (fs + (1, n_fs - 1)[way]) % n_fs, tp),
            device_id_type=MESH,
        )

    gu_side = functools.partial(side, gu_ref, gu_all, gu_send, gu_recv)
    dn_side = functools.partial(side, dn_ref, dn_all, dn_send, dn_recv)
    sc_side = functools.partial(side, ds_ref, sc_all, sc_send, sc_recv)

    def own_copies(make, way, act):
        @pl.when(fs < last if way == 0 else fs > 0)
        def _():
            act(make(fs, way, True))

    def start(copy):
        copy.start()

    def tok_copy(hop):
        peer = (me + hop) % peers
        return pltpu.make_async_remote_copy(
            src_ref=tok_ref,
            dst_ref=tok_all.at[pl.ds(pl.multiple_of(me * rows, rows), rows), :],
            send_sem=tok_send.at[peer],
            recv_sem=tok_recv.at[me],
            device_id=plane(peer),
            device_id_type=MESH,
        )

    def tok_arrival(peer):
        return pltpu.make_async_remote_copy(
            src_ref=tok_ref,
            dst_ref=tok_all.at[pl.ds(pl.multiple_of(peer * rows, rows), rows), :],
            send_sem=tok_send.at[peer],
            recv_sem=tok_recv.at[peer],
            device_id=plane(peer),
            device_id_type=MESH,
        )

    for way in (0, 1):
        own_copies(gu_side, way, start)
    for hop in range(1, peers):
        tok_copy(hop).start()
    for way in (0, 1):
        own_copies(sc_side, way, start)

    @pl.when(fs == 0)
    def _():
        own_copies(dn_side, 0, start)

    @pl.when(fs == last)
    def _():
        own_copies(dn_side, 1, start)

    tok_all[pl.ds(pl.multiple_of(me * rows, rows), rows), :] = tok_ref[...]

    def arrive(make, source, way):
        make(source, way, False).wait_recv()

        @pl.when(fs < last if way == 0 else fs > 0)
        def _():
            make(source, way, False).start()

    tile = 2 * rows
    tiles = peers // 2

    def gather_step(step):
        from_left, from_right = fs - step, fs + step

        @pl.when(from_left >= 0)
        def _():
            arrive(gu_side, from_left, 0)

            @pl.when(from_left == 0)
            def _():
                own_copies(dn_side, 0, start)

        @pl.when(from_right <= last)
        def _():
            arrive(gu_side, from_right, 1)

            @pl.when(from_right == last)
            def _():
                own_copies(dn_side, 1, start)

    def accumulate(source, weights, fresh):
        def body(j, carry):
            r = pl.ds(pl.multiple_of(j * tile, tile), tile)
            k = pl.ds(pl.multiple_of(source * depth, depth), depth)
            got = jnp.dot(tok_all[r, k], weights[...], preferred_element_type=jnp.float32)
            acc[r, :] = got if fresh else acc[r, :] + got
            return carry

        lax.fori_loop(0, tiles, body, 0)

    gather_step(1)
    for hop in range(1, peers):
        tok_arrival((me + hop) % peers).wait_recv()
    accumulate(fs, gu_ref, True)

    def gu_step(step, carry):
        @pl.when(step > 1)
        def _():
            gather_step(step)

        @pl.when(fs - step >= 0)
        def _():
            accumulate(fs - step, gu_all.at[fs - step], False)

        @pl.when(fs + step <= last)
        def _():
            accumulate(fs + step, gu_all.at[fs + step], False)

        return carry

    lax.fori_loop(1, n_fs, gu_step, 0)

    def activate(j, carry):
        r = pl.ds(pl.multiple_of(j * rows, rows), rows)
        both = acc[r, :]
        gate = both[:, :half] * gs_ref[...]
        up = both[:, half:] * us_ref[...]
        hidden[r, :] = (gate / (1.0 + jnp.exp(-gate)) * up).astype(jnp.bfloat16)
        return carry

    lax.fori_loop(0, peers, activate, 0)

    def part_copy(source, peer):
        return pltpu.make_async_remote_copy(
            src_ref=parts.at[source, pl.ds(pl.multiple_of(peer * rows, rows), rows), :],
            dst_ref=landed.at[source, me],
            send_sem=part_send.at[source, peer],
            recv_sem=part_recv.at[source, me],
            device_id=plane(peer),
            device_id_type=MESH,
        )

    def part_arrival(source, peer):
        return pltpu.make_async_remote_copy(
            src_ref=parts.at[source, pl.ds(pl.multiple_of(peer * rows, rows), rows), :],
            dst_ref=landed.at[source, peer],
            send_sem=part_send.at[source, peer],
            recv_sem=part_recv.at[source, peer],
            device_id=plane(peer),
            device_id_type=MESH,
        )

    def project(source, weights):
        def body(j, carry):
            r = pl.ds(pl.multiple_of(j * tile, tile), tile)
            parts[source, r, :] = jnp.dot(
                hidden[r, :], weights[...], preferred_element_type=jnp.float32
            ).astype(jnp.bfloat16)
            for k in (0, 1):
                peer = j * 2 + k

                @pl.when(peer != me)
                def _():
                    part_copy(source, peer).start()

            return carry

        lax.fori_loop(0, tiles, body, 0)

    def finish(source, scale):
        total = parts[source, pl.ds(pl.multiple_of(me * rows, rows), rows), :].astype(jnp.float32)

        def add(hop, total):
            peer = (me + hop) % peers
            part_arrival(source, peer).wait_recv()
            return total + landed[source, peer].astype(jnp.float32)

        for hop in range(1, peers):
            total = add(hop, total)
        out_ref[:, pl.ds(pl.multiple_of(source * cols, cols), cols)] = (total * scale).astype(
            jnp.bfloat16
        )

    project(fs, dn_ref)

    def dn_step(step, carry):
        from_left, from_right = fs - step, fs + step

        @pl.when(from_left >= 0)
        def _():
            arrive(sc_side, from_left, 0)
            arrive(dn_side, from_left, 0)

        @pl.when(from_right <= last)
        def _():
            arrive(sc_side, from_right, 1)
            arrive(dn_side, from_right, 1)

        @pl.when(from_left >= 0)
        def _():
            project(from_left, dn_all.at[from_left])

        @pl.when(from_right <= last)
        def _():
            project(from_right, dn_all.at[from_right])

        return carry

    lax.fori_loop(1, n_fs, dn_step, 0)

    finish(fs, ds_ref[0:1, :])

    def end_step(step, carry):
        for source in (fs - step, fs + step):

            @pl.when((source >= 0) & (source <= last))
            def _():
                finish(source, sc_all[source, 0:1, :])

        return carry

    lax.fori_loop(1, n_fs, end_step, 0)

    def sent_step(source, carry):
        for make in (gu_side, dn_side, sc_side):

            @pl.when((source <= fs) & (fs < last))
            def _():
                make(source, 0, False).wait_send()

            @pl.when((source >= fs) & (fs > 0))
            def _():
                make(source, 1, False).wait_send()

        for hop in range(1, peers):
            part_copy(source, (me + hop) % peers).wait_send()
        return carry

    lax.fori_loop(0, n_fs, sent_step, 0)
    for hop in range(1, peers):
        tok_copy(hop).wait_send()


def shards(
    sizes,
    tokens,
    norm_gain,
    gate_weight,
    gate_scale,
    up_weight,
    up_scale,
    down_weight,
    down_scale,
):
    n_rep, n_fs, n_tp = sizes
    peers = n_rep * n_tp
    width = gate_weight.shape[1] // n_rep
    begin = lax.axis_index("rep") * width

    def part(array, axis):
        return lax.dynamic_slice_in_dim(array, begin, width, axis)

    flat = tokens.astype(jnp.float32)
    mean_square = jnp.mean(flat * flat, axis=-1, keepdims=True)
    inverse = lax.rsqrt(mean_square + 1e-06)
    normed = (flat * inverse * norm_gain).astype(jnp.bfloat16)
    gu = jnp.concatenate(
        [part(gate_weight, 1).astype(jnp.bfloat16), part(up_weight, 1).astype(jnp.bfloat16)], axis=1
    )
    dn = part(down_weight, 0).astype(jnp.bfloat16)
    scale = jnp.broadcast_to(down_scale[None, :], (8, down_scale.shape[0]))
    rows, features = tokens.shape
    depth = gu.shape[0]
    cols = dn.shape[1]
    dma = pltpu.SemaphoreType.DMA
    vmem = pl.BlockSpec(memory_space=pltpu.VMEM)
    return pl.pallas_call(
        functools.partial(layer, n_rep, n_fs, n_tp),
        out_shape=jax.ShapeDtypeStruct((rows, features), jnp.bfloat16),
        in_specs=[vmem] * 6,
        out_specs=vmem,
        scratch_shapes=[
            pltpu.VMEM((peers * rows, features), jnp.bfloat16),
            pltpu.VMEM((n_fs, depth, 2 * width), jnp.bfloat16),
            pltpu.VMEM((n_fs, width, cols), jnp.bfloat16),
            pltpu.VMEM((n_fs, 8, cols), jnp.float32),
            pltpu.VMEM((peers * rows, 2 * width), jnp.float32),
            pltpu.VMEM((peers * rows, width), jnp.bfloat16),
            pltpu.VMEM((n_fs, peers * rows, cols), jnp.bfloat16),
            pltpu.VMEM((n_fs, peers, rows, cols), jnp.bfloat16),
            dma((peers,)),
            dma((peers,)),
            dma((2, n_fs)),
            dma((n_fs,)),
            dma((2, n_fs)),
            dma((n_fs,)),
            dma((2, n_fs)),
            dma((n_fs,)),
            dma((n_fs, peers)),
            dma((n_fs, peers)),
        ],
        compiler_params=pltpu.CompilerParams(
            collective_id=0, has_side_effects=True, vmem_limit_bytes=60 * 1024 * 1024
        ),
    )(normed, gu, dn, part(gate_scale, 0)[None, :], part(up_scale, 0)[None, :], scale)


def solution(mesh):
    in_specs = (
        P(("rep", "fs", "tp"), None),
        P(),
        P("fs", "tp"),
        P("tp"),
        P("fs", "tp"),
        P("tp"),
        P("tp", "fs"),
        P("fs"),
    )
    out_specs = P(("rep", "fs", "tp"), None)
    sizes = tuple(mesh.shape[axis] for axis in ("rep", "fs", "tp"))
    return jax.shard_map(
        functools.partial(shards, sizes),
        mesh=mesh,
        in_specs=in_specs,
        out_specs=out_specs,
        check_vma=False,
    )
```

time: 408 us -> 172 us (0.42)
  waiting for transfers between devices: 348 us -> 0 us
  Pallas kernels: 0 us -> 161 us
  matrix products: 21.7 us -> 0 us
  between operations: 13.2 us -> 0.07 us
  blocking collectives: 11.9 us -> 0 us
  other arithmetic: 12.9 us -> 2.74 us
  local copies, waits for them, and re-layouts: 0.03 us -> 7.51 us
    all_gather x4 -> x0, waiting for transfers between devices: 330 us -> none  [the longest x1 108 us: shards(): lax.all_gather(gate_low, 'fs', axis=0, tiled=True)]
    pallas_call x0 -> x1, Pallas kernels: none -> 161 us  [shards(): pl.pallas_call(functools.partial(layer, n_rep, n_fs, n_tp), out_shape=jax...]
    dot_general x2 -> x0, matrix products: 21.7 us -> none  [the longest x1 13.4 us: shards(): jnp.dot(hidden, down_full, preferred_element_type=jnp.float32)]
    reduce_scatter x1 -> x0, waiting for transfers between devices: 17.6 us -> none  [shards(): lax.psum_scatter(jnp.dot(hidden, down_full, preferred_element_type=jnp.fl...]
    all_gather x1 -> x0, blocking collectives: 11.9 us -> none  [shards(): scales = lax.all_gather(down_scale, 'fs', axis=0, tiled=True)]
    convert_element_type x4 -> x0, other arithmetic: 9.63 us -> none  [the longest x1 3.27 us: shards(): gate_low = gate_weight.astype(jnp.bfloat16)]
  transfers between devices with their start and end apart: 5 -> 0, of which waited for: 5 -> 0; matrix products, arithmetic and copies ran while one was open for 4% -> 0% of each run, Pallas kernels for 0% -> 0%
where the time goes in v2:
time: 172 us
  Pallas kernels  161 us (94%)
  local copies, waits for them, and re-layouts  7.51 us (4%)
  other arithmetic  2.74 us (2%)
    pallas_call x1, Pallas kernels, shards(): pl.pallas_call(functools.partial(layer, n_rep, n_fs, n_tp), out_shape=jax...  161 us

profile of v2, /device:TPU:0, one launch (start us, length us, event | category | flops | bytes accessed | tf_op | source)
XLA Modules:
  0.0 171.5 jit_solution(9737130286931609318)
XLA Ops:
  0.0 0.0 copy-start
  0.0 2.7 %dynamic-slice_convert_fusion = (bf16[512,704]{1,0:T(8,128)(2,1)S(1)}, bf16[512,704]{1,0:T(8,128)(2,1)S(1)}) fusion(f32[512,1408]{1,0:T(8,128)} %param.12, s32[]{:T(128)S(6)} %select_n.2, f32[512,1408]{1,0:T(8,128)} %param.10), kind=kLoop, calls=%fused_computation | loop fusion | bytes 2883588 | tf_op jit(solution)/shard_map/convert_element_type | solution.py:332
  2.7 0.0 copy-start.4
  2.7 0.0 copy-start.5
  2.7 0.0 copy-start.1
  2.7 0.0 copy-start.2
  2.8 0.0 copy-start.3
  2.8 1.6 pad_maximum_fusion.gu_ref
  4.3 0.0 copy-done
  4.3 1.0 dynamic-slice_convert_fusion.2.dn_ref
  5.3 0.0 copy-done.4
  5.3 0.1 dynamic_slice.18
  5.4 0.6 broadcast_in_dim.6.gs_ref
  6.0 0.0 copy-done.5
  6.0 0.1 dynamic_slice.19
  6.0 0.6 broadcast_in_dim.7.us_ref
  6.6 0.0 copy-done.1
  6.6 0.2 fusion
  6.8 0.0 copy-done.2
  6.8 1.0 fusion.2.tok_ref
  7.8 0.0 copy-done.3
  7.8 0.6 broadcast_in_dim.16.ds_ref
  8.4 161.2 %shard_map.82 = bf16[128,2048]{1,0:T(8,128)(2,1)} custom-call(bf16[128,2048]{1,0:T(8,128)(2,1)} %fusion.2.tok_ref, bf16[512,1408]{1,0:T(8,128)(2,1)} %pad_maximum_fusion.gu_ref, bf16[704,512]{1,0:T(8,128)(2,1)} %dynamic-slice_convert_fusion.2.dn_ref, f32[1,704]{1,0:T(1,128)} %broadcast_in_dim.6.gs_ref, f32[1,704]{1,0:T(1,128)} %broadcast_in_dim.7.us_ref, ...), custom_call_target="tpu_custom_call" | custom-call | tf_op jit(solution)/shard_map/pallas_call | solution.py:341
  169.7 1.9 %copy.10 = bf16[128,2048]{1,0:T(8,128)(2,1)} copy(bf16[128,2048]{1,0:T(8,128)(2,1)} %shard_map.82) | data formatting | bytes 1048576
  (1 shorter events, 0.0 us)
Async XLA Ops:
  0.0 4.3 %copy-start = (f32[1408,512]{1,0:T(8,128)S(1)}, f32[1408,512]{1,0:T(8,128)}, u32[]{:S(2)}) copy-start(f32[1408,512]{1,0:T(8,128)} %param.14) | copy-start | bytes 8650756
  2.7 2.6 %copy-start.4 = (f32[1408]{0:T(1024)S(1)}, f32[1408]{0:T(1024)}, u32[]{:S(2)}) copy-start(f32[1408]{0:T(1024)} %param.11) | copy-start | bytes 16900
  2.7 3.2 %copy-start.5 = (f32[1408]{0:T(1024)S(1)}, f32[1408]{0:T(1024)}, u32[]{:S(2)}) copy-start(f32[1408]{0:T(1024)} %param.13) | copy-start | bytes 16900
  2.7 3.9 %copy-start.1 = (bf16[128,2048]{1,0:T(8,128)(2,1)S(1)}, bf16[128,2048]{1,0:T(8,128)(2,1)}, u32[]{:S(2)}) copy-start(bf16[128,2048]{1,0:T(8,128)(2,1)} %param.8) | copy-start | bytes 1572868
  2.7 4.1 %copy-start.2 = (f32[2048]{0:T(1024)S(1)}, f32[2048]{0:T(1024)}, u32[]{:S(2)}) copy-start(f32[2048]{0:T(1024)} %param.9) | copy-start | bytes 24580
  2.8 5.1 %copy-start.3 = (f32[512]{0:T(512)S(1)}, f32[512]{0:T(512)}, u32[]{:S(2)}) copy-start(f32[512]{0:T(512)} %param.15) | copy-start | bytes 6148

commit v3 on v2

v3 whole, which is shorter than its diff:
```python
import functools

import jax
import jax.numpy as jnp
from jax import lax
from jax.experimental import pallas as pl
from jax.experimental.pallas import tpu as pltpu
from jax.sharding import PartitionSpec as P

MESH = pl.DeviceIdType.MESH


def layer(
    n_rep,
    n_fs,
    n_tp,
    tok_ref,
    gu_ref,
    dn_ref,
    hs_ref,
    ds_ref,
    out_ref,
    tok_all,
    gu_all,
    dn_all,
    sc_all,
    hs_all,
    acc,
    hidden,
    parts,
    landed,
    back,
    tok_send,
    tok_recv,
    gu_send,
    gu_recv,
    dn_send,
    dn_recv,
    sc_send,
    sc_recv,
    gu_sib_send,
    gu_sib_recv,
    dn_sib_send,
    dn_sib_recv,
    hs_sem,
    part_send,
    part_recv,
    back_send,
    back_recv,
    tok_z_send,
):
    rep, fs, tp = lax.axis_index("rep"), lax.axis_index("fs"), lax.axis_index("tp")
    n_row = n_tp // 2
    core = tp % 2
    chips = n_rep * n_row
    me = rep * n_row + tp // 2
    rows = tok_ref.shape[0]
    depth = gu_ref.shape[0]
    half = gu_ref.shape[1] // 2
    cols = dn_ref.shape[1]
    low, high, last = 1, n_fs - 2, n_fs - 1
    pair = fs // 2
    parity = fs % 2
    upper = jnp.where(pair < n_fs // 4, 0, 1)
    works = parity + upper == 1
    inside = (fs >= low) & (fs <= high)
    partner = (rep, fs + 1 - 2 * parity, tp)
    sibling = (rep, fs, tp + 1 - 2 * core)

    def chip(index):
        return (index // n_row, fs, (index % n_row) * 2 + core)

    barrier = pltpu.get_barrier_semaphore()
    for hop in (1, n_fs - 1):
        pl.semaphore_signal(
            barrier, inc=1, device_id=(rep, (fs + hop) % n_fs, tp), device_id_type=MESH
        )
    pl.semaphore_signal(barrier, inc=1, device_id=sibling, device_id_type=MESH)
    for hop in range(1, chips):
        pl.semaphore_signal(
            barrier, inc=1, device_id=chip((me + hop) % chips), device_id_type=MESH
        )
    pl.semaphore_wait(barrier, chips + 2)

    def remote(src, dst, send, recv, device):
        return pltpu.make_async_remote_copy(
            src_ref=src,
            dst_ref=dst,
            send_sem=send,
            recv_sem=recv,
            device_id=device,
            device_id_type=MESH,
        )

    def block(index):
        return pl.ds(pl.multiple_of(index * rows, rows), rows)

    def side(own, store, send, recv, source, way, first):
        return remote(
            own if first else store.at[source],
            store.at[source],
            send.at[way, source],
            recv.at[source],
            (rep, (fs + (1, n_fs - 1)[way]) % n_fs, tp),
        )

    gu_side = functools.partial(side, gu_ref, gu_all.at[0], gu_send, gu_recv)
    dn_side = functools.partial(side, dn_ref, dn_all.at[0], dn_send, dn_recv)
    sc_side = functools.partial(side, ds_ref, sc_all, sc_send, sc_recv)

    def sib(own, store, send, recv, source, first):
        return remote(
            own if first else store.at[0, source],
            store.at[1, source],
            send.at[source],
            recv.at[source],
            sibling,
        )

    gu_sib = functools.partial(sib, gu_ref, gu_all, gu_sib_send, gu_sib_recv)
    dn_sib = functools.partial(sib, dn_ref, dn_all, dn_sib_send, dn_sib_recv)
    hs_copy = remote(hs_ref, hs_all, hs_sem.at[0], hs_sem.at[1], sibling)

    def goes(way):
        return fs < high if way == 0 else fs > low

    def own_copies(make, way):
        @pl.when(goes(way))
        def _():
            make(fs, way, True).start()

    def tok_copy(plane, hop):
        to = (me + hop) % chips
        home = tok_all.at[block(plane * chips + me), :]
        return remote(
            tok_ref if plane == 0 else home,
            home,
            tok_send.at[plane, to],
            tok_recv.at[plane, me],
            chip(to),
        )

    def tok_arrival(plane, index):
        home = tok_all.at[block(plane * chips + index), :]
        return remote(
            home, home, tok_send.at[plane, index], tok_recv.at[plane, index], chip(index)
        )

    tok_z = remote(
        tok_ref, tok_all.at[block(chips + me), :], tok_z_send, tok_recv.at[1, me], partner
    )

    @pl.when(jnp.logical_not(works))
    def _():
        tok_z.start()

    for way in (0, 1):
        own_copies(gu_side, way)

    @pl.when(works)
    def _():
        for hop in range(1, chips):
            tok_copy(0, hop).start()
        hs_copy.start()
        gu_sib(fs, True).start()
        dn_sib(fs, True).start()

    for way in (0, 1):
        own_copies(sc_side, way)

    @pl.when(fs == 0)
    def _():
        own_copies(dn_side, 0)

    @pl.when(fs == last)
    def _():
        own_copies(dn_side, 1)

    @pl.when(works)
    def _():
        tok_all[block(me), :] = tok_ref[...]
        tok_z.wait_recv()
        for hop in range(1, chips):
            tok_copy(1, hop).start()

    def arrive(make, source, way, to_sibling):
        make(source, way, False).wait_recv()

        @pl.when(goes(way))
        def _():
            make(source, way, False).start()

        if to_sibling is not None:

            @pl.when(works)
            def _():
                to_sibling(source, False).start()

    tile = 2 * rows
    tiles = chips

    def left_ok(step):
        return inside & (fs - step >= 0)

    def right_ok(step):
        return inside & (fs + step <= last)

    def gather_step(step):
        from_left, from_right = fs - step, fs + step

        @pl.when(left_ok(step))
        def _():
            arrive(gu_side, from_left, 0, gu_sib)

            @pl.when(from_left == 0)
            def _():
                own_copies(dn_side, 0)

        @pl.when(right_ok(step))
        def _():
            arrive(gu_side, from_right, 1, gu_sib)

            @pl.when(from_right == last)
            def _():
                own_copies(dn_side, 1)

    def accumulate(source, weights, fresh):
        gu_sib(source, False).wait_recv()

        def body(j, carry):
            r = pl.ds(pl.multiple_of(j * tile, tile), tile)
            k = pl.ds(pl.multiple_of(source * depth, depth), depth)
            for c, block_of in ((0, weights), (1, gu_all.at[1, source])):
                got = jnp.dot(tok_all[r, k], block_of[...], preferred_element_type=jnp.float32)
                acc[c, r, :] = got if fresh else acc[c, r, :] + got
            return carry

        lax.fori_loop(0, tiles, body, 0)

    gather_step(1)

    @pl.when(works)
    def _():
        for hop in range(1, chips):
            for plane in (0, 1):
                tok_arrival(plane, (me + hop) % chips).wait_recv()
        accumulate(fs, gu_ref, True)

    def gu_step(step, carry):
        @pl.when(step > 1)
        def _():
            gather_step(step)

        @pl.when(works & left_ok(step))
        def _():
            accumulate(fs - step, gu_all.at[0, fs - step], False)

        @pl.when(works & right_ok(step))
        def _():
            accumulate(fs + step, gu_all.at[0, fs + step], False)

        return carry

    lax.fori_loop(1, n_fs, gu_step, 0)

    @pl.when(works)
    def _():
        hs_copy.wait_recv()

        def activate(j, carry):
            r = block(j)
            for c, scale in ((0, hs_ref), (1, hs_all)):
                both = acc[c, r, :] * scale[0:1, :]
                gate, up = both[:, :half], both[:, half:]
                hidden[c, r, :] = (gate / (1.0 + jnp.exp(-gate)) * up).astype(jnp.bfloat16)
            return carry

        lax.fori_loop(0, 2 * chips, activate, 0)

    def part_copy(source, plane, to):
        return remote(
            parts.at[source, block(plane * chips + to), :],
            landed.at[source, plane, me],
            part_send.at[source, plane, to],
            part_recv.at[source, plane, me],
            chip(to),
        )

    def part_arrival(source, plane, index):
        return remote(
            parts.at[source, block(plane * chips + index), :],
            landed.at[source, plane, index],
            part_send.at[source, plane, index],
            part_recv.at[source, plane, index],
            chip(index),
        )

    def project(source, weights):
        dn_sib(source, False).wait_recv()

        def body(i, carry):
            j = tiles - 1 - i
            r = pl.ds(pl.multiple_of(j * tile, tile), tile)
            parts[source, r, :] = (
                jnp.dot(hidden[0, r, :], weights[...], preferred_element_type=jnp.float32)
                + jnp.dot(
                    hidden[1, r, :], dn_all[1, source], preferred_element_type=jnp.float32
                )
            ).astype(jnp.bfloat16)
            for k in (0, 1):
                index = j * 2 + k

                @pl.when(index % chips != me)
                def _():
                    part_copy(source, index // chips, index % chips).start()

            return carry

        lax.fori_loop(0, tiles, body, 0)

    def back_copy(source):
        return remote(
            back.at[source], back.at[source], back_send.at[source], back_recv.at[source], partner
        )

    def finish(source, scale):
        for plane in (1, 0):
            total = parts[source, block(plane * chips + me), :].astype(jnp.float32)
            for hop in range(1, chips):
                index = (me + hop) % chips
                part_arrival(source, plane, index).wait_recv()
                total = total + landed[source, plane, index].astype(jnp.float32)
            mixed = (total * scale).astype(jnp.bfloat16)
            if plane == 1:
                back[source] = mixed
                back_copy(source).start()
            else:
                out_ref[:, pl.ds(pl.multiple_of(source * cols, cols), cols)] = mixed

    @pl.when(works)
    def _():
        project(fs, dn_ref)

    def dn_step(step, carry):
        from_left, from_right = fs - step, fs + step

        @pl.when(left_ok(step))
        def _():
            arrive(sc_side, from_left, 0, None)
            arrive(dn_side, from_left, 0, dn_sib)

        @pl.when(right_ok(step))
        def _():
            arrive(sc_side, from_right, 1, None)
            arrive(dn_side, from_right, 1, dn_sib)

        @pl.when(works & left_ok(step))
        def _():
            project(from_left, dn_all.at[0, from_left])

        @pl.when(works & right_ok(step))
        def _():
            project(from_right, dn_all.at[0, from_right])

        return carry

    lax.fori_loop(1, n_fs, dn_step, 0)

    @pl.when(works)
    def _():
        finish(fs, ds_ref[0:1, :])

    def end_step(step, carry):
        for source, ok in ((fs - step, left_ok(step)), (fs + step, right_ok(step))):

            @pl.when(works & ok)
            def _():
                finish(source, sc_all[source, 0:1, :])

        return carry

    lax.fori_loop(1, n_fs, end_step, 0)

    @pl.when(jnp.logical_not(works))
    def _():
        tok_z.wait_send()

        def take(source, carry):
            back_copy(source).wait_recv()
            out_ref[:, pl.ds(pl.multiple_of(source * cols, cols), cols)] = back[source]
            return carry

        lax.fori_loop(0, n_fs, take, 0)

    def sent_step(source, carry):
        for make in (gu_side, dn_side, sc_side):

            @pl.when((source <= fs) & goes(0))
            def _():
                make(source, 0, False).wait_send()

            @pl.when((source >= fs) & goes(1))
            def _():
                make(source, 1, False).wait_send()

        @pl.when(works)
        def _():
            gu_sib(source, False).wait_send()
            dn_sib(source, False).wait_send()
            back_copy(source).wait_send()
            for hop in range(1, chips):
                for plane in (0, 1):
                    part_copy(source, plane, (me + hop) % chips).wait_send()

        return carry

    lax.fori_loop(0, n_fs, sent_step, 0)

    @pl.when(works)
    def _():
        hs_copy.wait_send()
        for hop in range(1, chips):
            for plane in (0, 1):
                tok_copy(plane, hop).wait_send()


def shards(
    sizes,
    tokens,
    norm_gain,
    gate_weight,
    gate_scale,
    up_weight,
    up_scale,
    down_weight,
    down_scale,
):
    n_rep, n_fs, n_tp = sizes
    chips = n_rep * n_tp // 2
    width = gate_weight.shape[1] // n_rep
    begin = lax.axis_index("rep") * width

    def part(array, axis):
        return lax.dynamic_slice_in_dim(array, begin, width, axis)

    flat = tokens.astype(jnp.float32)
    mean_square = jnp.mean(flat * flat, axis=-1, keepdims=True)
    inverse = lax.rsqrt(mean_square + 1e-06)
    normed = (flat * inverse * norm_gain).astype(jnp.bfloat16)
    gu = jnp.concatenate(
        [part(gate_weight, 1).astype(jnp.bfloat16), part(up_weight, 1).astype(jnp.bfloat16)], axis=1
    )
    dn = part(down_weight, 0).astype(jnp.bfloat16)
    scale = jnp.broadcast_to(down_scale[None, :], (8, down_scale.shape[0]))
    hidden_scale = jnp.concatenate([part(gate_scale, 0), part(up_scale, 0)])
    hidden_scale = jnp.broadcast_to(hidden_scale[None, :], (8, 2 * width))
    rows, features = tokens.shape
    depth = gu.shape[0]
    cols = dn.shape[1]
    dma = pltpu.SemaphoreType.DMA
    vmem = pl.BlockSpec(memory_space=pltpu.VMEM)
    return pl.pallas_call(
        functools.partial(layer, n_rep, n_fs, n_tp),
        out_shape=jax.ShapeDtypeStruct((rows, features), jnp.bfloat16),
        in_specs=[vmem] * 5,
        out_specs=vmem,
        scratch_shapes=[
            pltpu.VMEM((2 * chips * rows, features), jnp.bfloat16),
            pltpu.VMEM((2, n_fs, depth, 2 * width), jnp.bfloat16),
            pltpu.VMEM((2, n_fs, width, cols), jnp.bfloat16),
            pltpu.VMEM((n_fs, 8, cols), jnp.float32),
            pltpu.VMEM((8, 2 * width), jnp.float32),
            pltpu.VMEM((2, 2 * chips * rows, 2 * width), jnp.float32),
            pltpu.VMEM((2, 2 * chips * rows, width), jnp.bfloat16),
            pltpu.VMEM((n_fs, 2 * chips * rows, cols), jnp.bfloat16),
            pltpu.VMEM((n_fs, 2, chips, rows, cols), jnp.bfloat16),
            pltpu.VMEM((n_fs, rows, cols), jnp.bfloat16),
            dma((2, chips)),
            dma((2, chips)),
            dma((2, n_fs)),
            dma((n_fs,)),
            dma((2, n_fs)),
            dma((n_fs,)),
            dma((2, n_fs)),
            dma((n_fs,)),
            dma((n_fs,)),
            dma((n_fs,)),
            dma((n_fs,)),
            dma((n_fs,)),
            dma((2,)),
            dma((n_fs, 2, chips)),
            dma((n_fs, 2, chips)),
            dma((n_fs,)),
            dma((n_fs,)),
            dma,
        ],
        compiler_params=pltpu.CompilerParams(
            collective_id=0, has_side_effects=True, vmem_limit_bytes=60 * 1024 * 1024
        ),
    )(normed, gu, dn, hidden_scale, scale)


def solution(mesh):
    in_specs = (
        P(("rep", "fs", "tp"), None),
        P(),
        P("fs", "tp"),
        P("tp"),
        P("fs", "tp"),
        P("tp"),
        P("tp", "fs"),
        P("fs"),
    )
    out_specs = P(("rep", "fs", "tp"), None)
    sizes = tuple(mesh.shape[axis] for axis in ("rep", "fs", "tp"))
    return jax.shard_map(
        functools.partial(shards, sizes),
        mesh=mesh,
        in_specs=in_specs,
        out_specs=out_specs,
        check_vma=False,
    )
```

time: 172 us -> 152 us (0.88)
  the two profiles are of different devices: /device:TPU:0 before, /device:TPU:1 now
where the time goes in v3:
time: 152 us
  Pallas kernels  142 us (93%)
  local copies, waits for them, and re-layouts  6.94 us (5%)
  other arithmetic  2.82 us (2%)
    pallas_call x1, Pallas kernels, shards(): pl.pallas_call(functools.partial(layer, n_rep, n_fs, n_tp), out_shape=jax...  142 us

profile of v3, /device:TPU:1, one launch (start us, length us, event | category | flops | bytes accessed | tf_op | source)
XLA Modules:
  0.0 151.8 jit_solution(9632950537022280153)
XLA Ops:
  0.0 0.0 copy-start
  0.0 0.0 copy-start.4
  0.0 0.0 copy-start.5
  0.0 2.7 %dynamic-slice_convert_fusion = (bf16[512,704]{1,0:T(8,128)(2,1)S(1)}, bf16[512,704]{1,0:T(8,128)(2,1)S(1)}) fusion(f32[512,1408]{1,0:T(8,128)} %param.12, s32[]{:T(128)S(6)} %select_n.2, f32[512,1408]{1,0:T(8,128)} %param.10), kind=kLoop, calls=%fused_computation | loop fusion | bytes 2883588 | tf_op jit(solution)/shard_map/convert_element_type | solution.py:451
  2.7 0.0 copy-start.1
  2.7 0.0 copy-start.2
  2.7 0.0 copy-start.3
  2.8 1.6 %pad_maximum_fusion.gu_ref = bf16[512,1408]{1,0:T(8,128)(2,1)} fusion(bf16[512,704]{1,0:T(8,128)(2,1)S(1)} %get-tuple-element.5, bf16[512,704]{1,0:T(8,128)(2,1)S(1)} %get-tuple-element.6), kind=kLoop, calls=%fused_computation.2 | loop fusion | flops 2883584 | bytes 2883584 | tf_op jit(solution)/shard_map/concatenate | solution.py:450
  4.3 0.0 copy-done.4
  4.3 0.1 dynamic_slice.18
  4.4 0.0 copy-done.5
  4.4 0.1 dynamic_slice.19
  4.5 0.1 pad_maximum_fusion.1
  4.6 0.6 broadcast_in_dim.4.hs_ref
  5.2 0.0 copy-done
  5.2 1.0 dynamic-slice_convert_fusion.2.dn_ref
  6.1 0.0 copy-done.1
  6.1 0.2 fusion
  6.3 0.0 copy-done.2
  6.3 1.0 fusion.2.tok_ref
  7.3 0.0 copy-done.3
  7.3 0.6 broadcast_in_dim.5.ds_ref
  7.9 142.0 %shard_map.82 = bf16[128,2048]{1,0:T(8,128)(2,1)} custom-call(bf16[128,2048]{1,0:T(8,128)(2,1)} %fusion.2.tok_ref, bf16[512,1408]{1,0:T(8,128)(2,1)} %pad_maximum_fusion.gu_ref, bf16[704,512]{1,0:T(8,128)(2,1)} %dynamic-slice_convert_fusion.2.dn_ref, f32[8,1408]{1,0:T(8,128)} %broadcast_in_dim.4.hs_ref, f32[8,512]{1,0:T(8,128)} %broadcast_in_dim.5.ds_ref), custom_call_target="tpu_custom_call" | custom-call | tf_op jit(solution)/shard_map/pallas_call | solution.py:462
  150.0 1.9 %copy.10 = bf16[128,2048]{1,0:T(8,128)(2,1)} copy(bf16[128,2048]{1,0:T(8,128)(2,1)} %shard_map.82) | data formatting | bytes 1048576
  (1 shorter events, 0.0 us)
Async XLA Ops:
  0.0 5.2 %copy-start = (f32[1408,512]{1,0:T(8,128)S(1)}, f32[1408,512]{1,0:T(8,128)}, u32[]{:S(2)}) copy-start(f32[1408,512]{1,0:T(8,128)} %param.14) | copy-start | bytes 8650756
  0.0 4.3 %copy-start.4 = (f32[1408]{0:T(1024)S(1)}, f32[1408]{0:T(1024)}, u32[]{:S(2)}) copy-start(f32[1408]{0:T(1024)} %param.11) | copy-start | bytes 16900
  0.0 4.4 %copy-start.5 = (f32[1408]{0:T(1024)S(1)}, f32[1408]{0:T(1024)}, u32[]{:S(2)}) copy-start(f32[1408]{0:T(1024)} %param.13) | copy-start | bytes 16900
  2.7 3.4 %copy-start.1 = (bf16[128,2048]{1,0:T(8,128)(2,1)S(1)}, bf16[128,2048]{1,0:T(8,128)(2,1)}, u32[]{:S(2)}) copy-start(bf16[128,2048]{1,0:T(8,128)(2,1)} %param.8) | copy-start | bytes 1572868
  2.7 3.6 %copy-start.2 = (f32[2048]{0:T(1024)S(1)}, f32[2048]{0:T(1024)}, u32[]{:S(2)}) copy-start(f32[2048]{0:T(1024)} %param.9) | copy-start | bytes 24580
  2.7 4.6 %copy-start.3 = (f32[512]{0:T(512)S(1)}, f32[512]{0:T(512)}, u32[]{:S(2)}) copy-start(f32[512]{0:T(512)} %param.15) | copy-start | bytes 6148

commit v4 on v3

--- a/solution.py
+++ b/solution.py
@@ -55,8 +55,9 @@
     chips = n_rep * n_row
     me = rep * n_row + tp // 2
     rows = tok_ref.shape[0]
-    depth = gu_ref.shape[0]
-    half = gu_ref.shape[1] // 2
+    pieces = gu_ref.shape[0]
+    depth = gu_ref.shape[1]
+    half = gu_ref.shape[2] // 2
     cols = dn_ref.shape[1]
     low, high, last = 1, n_fs - 2, n_fs - 1
     pair = fs // 2
@@ -104,7 +105,16 @@
             (rep, (fs + (1, n_fs - 1)[way]) % n_fs, tp),
         )
 
-    gu_side = functools.partial(side, gu_ref, gu_all.at[0], gu_send, gu_recv)
+    def gu_side(piece, source, way, first):
+        unit = source * pieces + piece
+        return remote(
+            gu_ref.at[piece] if first else gu_all.at[0, unit],
+            gu_all.at[0, unit],
+            gu_send.at[way, unit],
+            gu_recv.at[unit],
+            (rep, (fs + (1, n_fs - 1)[way]) % n_fs, tp),
+        )
+
     dn_side = functools.partial(side, dn_ref, dn_all.at[0], dn_send, dn_recv)
     sc_side = functools.partial(side, ds_ref, sc_all, sc_send, sc_recv)
 
@@ -117,7 +127,13 @@
             sibling,
         )
 
-    gu_sib = functools.partial(sib, gu_ref, gu_all, gu_sib_send, gu_sib_recv)
+    def gu_sib(piece, source, first):
+        unit = source * pieces + piece
+        return sib(gu_ref.at[piece], gu_all, gu_sib_send, gu_sib_recv, unit, first)
+
+    def gu_part(piece):
+        return functools.partial(gu_side, piece), functools.partial(gu_sib, piece)
+
     dn_sib = functools.partial(sib, dn_ref, dn_all, dn_sib_send, dn_sib_recv)
     hs_copy = remote(hs_ref, hs_all, hs_sem.at[0], hs_sem.at[1], sibling)
 
@@ -150,19 +166,22 @@
         tok_ref, tok_all.at[block(chips + me), :], tok_z_send, tok_recv.at[1, me], partner
     )
 
-    @pl.when(jnp.logical_not(works))
-    def _():
-        tok_z.start()
-
-    for way in (0, 1):
-        own_copies(gu_side, way)
+    for piece in range(pieces):
+        for way in (0, 1):
+            own_copies(gu_part(piece)[0], way)
+        if piece == 0:
+
+            @pl.when(jnp.logical_not(works))
+            def _():
+                tok_z.start()
 
     @pl.when(works)
     def _():
         for hop in range(1, chips):
             tok_copy(0, hop).start()
         hs_copy.start()
-        gu_sib(fs, True).start()
+        for piece in range(pieces):
+            gu_sib(piece, fs, True).start()
         dn_sib(fs, True).start()
 
     for way in (0, 1):
@@ -205,59 +224,67 @@
     def right_ok(step):
         return inside & (fs + step <= last)
 
-    def gather_step(step):
+    def gather_step(step, piece):
         from_left, from_right = fs - step, fs + step
+        move, share = gu_part(piece)
 
         @pl.when(left_ok(step))
         def _():
-            arrive(gu_side, from_left, 0, gu_sib)
-
-            @pl.when(from_left == 0)
-            def _():
-                own_copies(dn_side, 0)
+            arrive(move, from_left, 0, share)
+
+            if piece == pieces - 1:
+
+                @pl.when(from_left == 0)
+                def _():
+                    own_copies(dn_side, 0)
 
         @pl.when(right_ok(step))
         def _():
-            arrive(gu_side, from_right, 1, gu_sib)
-
-            @pl.when(from_right == last)
-            def _():
-                own_copies(dn_side, 1)
-
-    def accumulate(source, weights, fresh):
-        gu_sib(source, False).wait_recv()
+            arrive(move, from_right, 1, share)
+
+            if piece == pieces - 1:
+
+                @pl.when(from_right == last)
+                def _():
+                    own_copies(dn_side, 1)
+
+    def accumulate(piece, source, weights, fresh):
+        gu_sib(piece, source, False).wait_recv()
+        unit = source * pieces + piece
 
         def body(j, carry):
             r = pl.ds(pl.multiple_of(j * tile, tile), tile)
-            k = pl.ds(pl.multiple_of(source * depth, depth), depth)
-            for c, block_of in ((0, weights), (1, gu_all.at[1, source])):
+            k = pl.ds(pl.multiple_of(unit * depth, depth), depth)
+            for c, block_of in ((0, weights), (1, gu_all.at[1, unit])):
                 got = jnp.dot(tok_all[r, k], block_of[...], preferred_element_type=jnp.float32)
                 acc[c, r, :] = got if fresh else acc[c, r, :] + got
             return carry
 
         lax.fori_loop(0, tiles, body, 0)
 
-    gather_step(1)
+    for piece in range(pieces):
+        gather_step(1, piece)
 
     @pl.when(works)
     def _():
         for hop in range(1, chips):
             for plane in (0, 1):
                 tok_arrival(plane, (me + hop) % chips).wait_recv()
-        accumulate(fs, gu_ref, True)
+        for piece in range(pieces):
+            accumulate(piece, fs, gu_ref.at[piece], piece == 0)
 
     def gu_step(step, carry):
-        @pl.when(step > 1)
-        def _():
-            gather_step(step)
-
-        @pl.when(works & left_ok(step))
-        def _():
-            accumulate(fs - step, gu_all.at[0, fs - step], False)
-
-        @pl.when(works & right_ok(step))
-        def _():
-            accumulate(fs + step, gu_all.at[0, fs + step], False)
+        for piece in range(pieces):
+
+            @pl.when(step > 1)
+            def _():
+                gather_step(step, piece)
+
+            for source, ok in ((fs - step, left_ok(step)), (fs + step, right_ok(step))):
+
+                @pl.when(works & ok)
+                def _():
+                    accumulate(piece, source, gu_all.at[0, source * pieces + piece], False)
 
         return carry
 
@@ -393,7 +420,7 @@
         lax.fori_loop(0, n_fs, take, 0)
 
     def sent_step(source, carry):
-        for make in (gu_side, dn_side, sc_side):
+        for make in [gu_part(piece)[0] for piece in range(pieces)] + [dn_side, sc_side]:
 
             @pl.when((source <= fs) & goes(0))
             def _():
@@ -405,7 +432,8 @@
 
         @pl.when(works)
         def _():
-            gu_sib(source, False).wait_send()
+            for piece in range(pieces):
+                gu_sib(piece, source, False).wait_send()
             dn_sib(source, False).wait_send()
             back_copy(source).wait_send()
             for hop in range(1, chips):
@@ -455,7 +483,9 @@
     hidden_scale = jnp.concatenate([part(gate_scale, 0), part(up_scale, 0)])
     hidden_scale = jnp.broadcast_to(hidden_scale[None, :], (8, 2 * width))
     rows, features = tokens.shape
-    depth = gu.shape[0]
+    pieces = 2 if gu.shape[0] % 256 == 0 else 1
+    depth = gu.shape[0] // pieces
+    gu = gu.reshape(pieces, depth, 2 * width)
     cols = dn.shape[1]
     dma = pltpu.SemaphoreType.DMA
     vmem = pl.BlockSpec(memory_space=pltpu.VMEM)
@@ -466,7 +496,7 @@
         out_specs=vmem,
         scratch_shapes=[
             pltpu.VMEM((2 * chips * rows, features), jnp.bfloat16),
-            pltpu.VMEM((2, n_fs, depth, 2 * width), jnp.bfloat16),
+            pltpu.VMEM((2, n_fs * pieces, depth, 2 * width), jnp.bfloat16),
             pltpu.VMEM((2, n_fs, width, cols), jnp.bfloat16),
             pltpu.VMEM((n_fs, 8, cols), jnp.float32),
             pltpu.VMEM((8, 2 * width), jnp.float32),
@@ -477,14 +507,14 @@
             pltpu.VMEM((n_fs, rows, cols), jnp.bfloat16),
             dma((2, chips)),
             dma((2, chips)),
+            dma((2, n_fs * pieces)),
+            dma((n_fs * pieces,)),
             dma((2, n_fs)),
             dma((n_fs,)),
             dma((2, n_fs)),
             dma((n_fs,)),
-            dma((2, n_fs)),
-            dma((n_fs,)),
-            dma((n_fs,)),
-            dma((n_fs,)),
+            dma((n_fs * pieces,)),
+            dma((n_fs * pieces,)),
             dma((n_fs,)),
             dma((n_fs,)),
             dma((2,)),

time: 152 us -> 144 us (0.947)
  the two profiles are of different devices: /device:TPU:1 before, /device:TPU:0 now
where the time goes in v4:
time: 144 us
  Pallas kernels  134 us (93%)
  local copies, waits for them, and re-layouts  6.93 us (5%)
  other arithmetic  2.82 us (2%)
    pallas_call x1, Pallas kernels, shards(): pl.pallas_call(functools.partial(layer, n_rep, n_fs, n_tp), out_shape=jax...  134 us

profile of v4, /device:TPU:0, one launch (start us, length us, event | category | flops | bytes accessed | tf_op | source)
XLA Modules:
  0.0 144.1 jit_solution(8103731280160613802)
XLA Ops:
  0.0 0.0 copy-start
  0.0 0.0 copy-start.4
  0.0 0.0 copy-start.5
  0.0 2.7 %dynamic-slice_convert_fusion = (bf16[512,704]{1,0:T(8,128)(2,1)S(1)}, bf16[512,704]{1,0:T(8,128)(2,1)S(1)}) fusion(f32[512,1408]{1,0:T(8,128)} %param.12, s32[]{:T(128)S(6)} %select_n.2, f32[512,1408]{1,0:T(8,128)} %param.10), kind=kLoop, calls=%fused_computation | loop fusion | bytes 2883588 | tf_op jit(solution)/shard_map/convert_element_type | solution.py:479
  2.7 0.0 copy-start.1
  2.7 0.0 copy-start.2
  2.7 0.0 copy-start.3
  2.7 1.6 %pad_maximum_fusion = bf16[512,1408]{1,0:T(8,128)(2,1)} fusion(bf16[512,704]{1,0:T(8,128)(2,1)S(1)} %get-tuple-element.5, bf16[512,704]{1,0:T(8,128)(2,1)S(1)} %get-tuple-element.6), kind=kLoop, calls=%fused_computation.2 | loop fusion | flops 2883584 | bytes 2883584 | tf_op jit(solution)/shard_map/concatenate | solution.py:478
  4.3 0.0 copy-done.4
  4.3 0.1 dynamic_slice.18
  4.4 0.0 copy-done.5
  4.4 0.1 dynamic_slice.19
  4.5 0.1 pad_maximum_fusion.1
  4.5 0.6 broadcast_in_dim.4.hs_ref
  5.2 0.0 copy-done
  5.2 1.0 dynamic-slice_convert_fusion.2.dn_ref
  6.1 0.0 copy-done.1
  6.1 0.2 fusion
  6.3 0.0 copy-done.2
  6.3 1.0 fusion.2.tok_ref
  7.3 0.0 copy-done.3
  7.3 0.6 broadcast_in_dim.5.ds_ref
  7.9 134.3 %shard_map.82 = bf16[128,2048]{1,0:T(8,128)(2,1)} custom-call(bf16[128,2048]{1,0:T(8,128)(2,1)} %fusion.2.tok_ref, bf16[2,256,1408]{2,1,0:T(8,128)(2,1)} %bitcast.1, bf16[704,512]{1,0:T(8,128)(2,1)} %dynamic-slice_convert_fusion.2.dn_ref, f32[8,1408]{1,0:T(8,128)} %broadcast_in_dim.4.hs_ref, f32[8,512]{1,0:T(8,128)} %broadcast_in_dim.5.ds_ref), custom_call_target="tpu_custom_call" | custom-call | tf_op jit(solution)/shard_map/pallas_call | solution.py:492
  142.2 1.9 %copy.10 = bf16[128,2048]{1,0:T(8,128)(2,1)} copy(bf16[128,2048]{1,0:T(8,128)(2,1)} %shard_map.82) | data formatting | bytes 1048576
  (1 shorter events, 0.0 us)
Async XLA Ops:
  0.0 5.2 %copy-start = (f32[1408,512]{1,0:T(8,128)S(1)}, f32[1408,512]{1,0:T(8,128)}, u32[]{:S(2)}) copy-start(f32[1408,512]{1,0:T(8,128)} %param.14) | copy-start | bytes 8650756
  0.0 4.3 %copy-start.4 = (f32[1408]{0:T(1024)S(1)}, f32[1408]{0:T(1024)}, u32[]{:S(2)}) copy-start(f32[1408]{0:T(1024)} %param.11) | copy-start | bytes 16900
  0.0 4.4 %copy-start.5 = (f32[1408]{0:T(1024)S(1)}, f32[1408]{0:T(1024)}, u32[]{:S(2)}) copy-start(f32[1408]{0:T(1024)} %param.13) | copy-start | bytes 16900
  2.7 3.4 %copy-start.1 = (bf16[128,2048]{1,0:T(8,128)(2,1)S(1)}, bf16[128,2048]{1,0:T(8,128)(2,1)}, u32[]{:S(2)}) copy-start(bf16[128,2048]{1,0:T(8,128)(2,1)} %param.8) | copy-start | bytes 1572868
  2.7 3.6 %copy-start.2 = (f32[2048]{0:T(1024)S(1)}, f32[2048]{0:T(1024)}, u32[]{:S(2)}) copy-start(f32[2048]{0:T(1024)} %param.9) | copy-start | bytes 24580
  2.7 4.6 %copy-start.3 = (f32[512]{0:T(512)S(1)}, f32[512]{0:T(512)}, u32[]{:S(2)}) copy-start(f32[512]{0:T(512)} %param.15) | copy-start | bytes 6148

commit v5 on v4

--- a/solution.py
+++ b/solution.py
@@ -290,19 +290,12 @@
 
     lax.fori_loop(1, n_fs, gu_step, 0)
 
-    @pl.when(works)
-    def _():
-        hs_copy.wait_recv()
-
-        def activate(j, carry):
-            r = block(j)
-            for c, scale in ((0, hs_ref), (1, hs_all)):
-                both = acc[c, r, :] * scale[0:1, :]
-                gate, up = both[:, :half], both[:, half:]
-                hidden[c, r, :] = (gate / (1.0 + jnp.exp(-gate)) * up).astype(jnp.bfloat16)
-            return carry
-
-        lax.fori_loop(0, 2 * chips, activate, 0)
+    def activate(index):
+        r = block(index)
+        for c, scale in ((0, hs_ref), (1, hs_all)):
+            both = acc[c, r, :] * scale[0:1, :]
+            gate, up = both[:, :half], both[:, half:]
+            hidden[c, r, :] = (gate / (1.0 + jnp.exp(-gate)) * up).astype(jnp.bfloat16)
 
     def part_copy(source, plane, to):
         return remote(
@@ -322,12 +315,15 @@
             chip(index),
         )
 
-    def project(source, weights):
+    def project(source, weights, fresh):
         dn_sib(source, False).wait_recv()
 
         def body(i, carry):
             j = tiles - 1 - i
             r = pl.ds(pl.multiple_of(j * tile, tile), tile)
+            if fresh:
+                for k in (0, 1):
+                    activate(j * 2 + k)
             parts[source, r, :] = (
                 jnp.dot(hidden[0, r, :], weights[...], preferred_element_type=jnp.float32)
                 + jnp.dot(
@@ -366,7 +362,8 @@
 
     @pl.when(works)
     def _():
-        project(fs, dn_ref)
+        hs_copy.wait_recv()
+        project(fs, dn_ref, True)
 
     def dn_step(step, carry):
         from_left, from_right = fs - step, fs + step
@@ -383,11 +380,11 @@
 
         @pl.when(works & left_ok(step))
         def _():
-            project(from_left, dn_all.at[0, from_left])
+            project(from_left, dn_all.at[0, from_left], False)
 
         @pl.when(works & right_ok(step))
         def _():
-            project(from_right, dn_all.at[0, from_right])
+            project(from_right, dn_all.at[0, from_right], False)
 
         return carry
 

time: 144 us -> 143 us (level)
  no operation moved by 1% of the time
where the time goes in v5:
time: 143 us
  Pallas kernels  133 us (93%)
  local copies, waits for them, and re-layouts  6.93 us (5%)
  other arithmetic  2.82 us (2%)
    pallas_call x1, Pallas kernels, shards(): pl.pallas_call(functools.partial(layer, n_rep, n_fs, n_tp), out_shape=jax...  133 us

profile of v5, /device:TPU:0, one launch (start us, length us, event | category | flops | bytes accessed | tf_op | source)
XLA Modules:
  0.0 142.8 jit_solution(1903678663071677420)
XLA Ops:
  0.0 0.0 copy-start
  0.0 0.0 copy-start.4
  0.0 0.0 copy-start.5
  0.0 2.7 %dynamic-slice_convert_fusion = (bf16[512,704]{1,0:T(8,128)(2,1)S(1)}, bf16[512,704]{1,0:T(8,128)(2,1)S(1)}) fusion(f32[512,1408]{1,0:T(8,128)} %param.12, s32[]{:T(128)S(6)} %select_n.2, f32[512,1408]{1,0:T(8,128)} %param.10), kind=kLoop, calls=%fused_computation | loop fusion | bytes 2883588 | tf_op jit(solution)/shard_map/convert_element_type | solution.py:476
  2.7 0.0 copy-start.1
  2.7 0.0 copy-start.2
  2.7 0.0 copy-start.3
  2.7 1.6 %pad_maximum_fusion = bf16[512,1408]{1,0:T(8,128)(2,1)} fusion(bf16[512,704]{1,0:T(8,128)(2,1)S(1)} %get-tuple-element.5, bf16[512,704]{1,0:T(8,128)(2,1)S(1)} %get-tuple-element.6), kind=kLoop, calls=%fused_computation.2 | loop fusion | flops 2883584 | bytes 2883584 | tf_op jit(solution)/shard_map/concatenate | solution.py:475
  4.3 0.0 copy-done.4
  4.3 0.1 dynamic_slice.18
  4.4 0.0 copy-done.5
  4.4 0.1 dynamic_slice.19
  4.5 0.1 pad_maximum_fusion.1
  4.5 0.6 broadcast_in_dim.4.hs_ref
  5.2 0.0 copy-done
  5.2 1.0 dynamic-slice_convert_fusion.2.dn_ref
  6.1 0.0 copy-done.1
  6.1 0.2 fusion
  6.3 0.0 copy-done.2
  6.3 1.0 fusion.2.tok_ref
  7.3 0.0 copy-done.3
  7.3 0.6 broadcast_in_dim.5.ds_ref
  7.9 133.0 %shard_map.82 = bf16[128,2048]{1,0:T(8,128)(2,1)} custom-call(bf16[128,2048]{1,0:T(8,128)(2,1)} %fusion.2.tok_ref, bf16[2,256,1408]{2,1,0:T(8,128)(2,1)} %bitcast.1, bf16[704,512]{1,0:T(8,128)(2,1)} %dynamic-slice_convert_fusion.2.dn_ref, f32[8,1408]{1,0:T(8,128)} %broadcast_in_dim.4.hs_ref, f32[8,512]{1,0:T(8,128)} %broadcast_in_dim.5.ds_ref), custom_call_target="tpu_custom_call" | custom-call | tf_op jit(solution)/shard_map/pallas_call | solution.py:489
  140.9 1.9 %copy.10 = bf16[128,2048]{1,0:T(8,128)(2,1)} copy(bf16[128,2048]{1,0:T(8,128)(2,1)} %shard_map.82) | data formatting | bytes 1048576
  (1 shorter events, 0.0 us)
Async XLA Ops:
  0.0 5.2 %copy-start = (f32[1408,512]{1,0:T(8,128)S(1)}, f32[1408,512]{1,0:T(8,128)}, u32[]{:S(2)}) copy-start(f32[1408,512]{1,0:T(8,128)} %param.14) | copy-start | bytes 8650756
  0.0 4.3 %copy-start.4 = (f32[1408]{0:T(1024)S(1)}, f32[1408]{0:T(1024)}, u32[]{:S(2)}) copy-start(f32[1408]{0:T(1024)} %param.11) | copy-start | bytes 16900
  0.0 4.4 %copy-start.5 = (f32[1408]{0:T(1024)S(1)}, f32[1408]{0:T(1024)}, u32[]{:S(2)}) copy-start(f32[1408]{0:T(1024)} %param.13) | copy-start | bytes 16900
  2.7 3.4 %copy-start.1 = (bf16[128,2048]{1,0:T(8,128)(2,1)S(1)}, bf16[128,2048]{1,0:T(8,128)(2,1)}, u32[]{:S(2)}) copy-start(bf16[128,2048]{1,0:T(8,128)(2,1)} %param.8) | copy-start | bytes 1572868
  2.7 3.6 %copy-start.2 = (f32[2048]{0:T(1024)S(1)}, f32[2048]{0:T(1024)}, u32[]{:S(2)}) copy-start(f32[2048]{0:T(1024)} %param.9) | copy-start | bytes 24580
  2.7 4.6 %copy-start.3 = (f32[512]{0:T(512)S(1)}, f32[512]{0:T(512)}, u32[]{:S(2)}) copy-start(f32[512]{0:T(512)} %param.15) | copy-start | bytes 6148
